TPU v7x, 512 devices: a whole 4x8x8 slice. The times are simulated.
512 devices in a mesh: kv: 128 (over z, y, core), tp: 4 (over x).
Axes of the slice: x: 4, y: 8, z: 8, core: 2. Of those that a mesh axis runs over, the one named last changes fastest.
Arguments:
- hidden: bfloat16 [128, 4096], P(None, 'tp'), may hold values from -50 to 50
- input_gain: bfloat16 [4096], P('tp'), may hold values from 0.099609375 to 1.8984375
- x_weight: bfloat16 [4096, 8192], P('tp', 'kv'), may hold values from -0.09375 to 0.09375
- z_weight: bfloat16 [4096, 8192], P('tp', 'kv'), may hold values from -0.09375 to 0.09375
- bc_weight: bfloat16 [4096, 8192], P('tp', 'kv'), may hold values from -0.09375 to 0.09375
- dt_weight: bfloat16 [4096, 128], P('tp', 'kv'), may hold values from -0.09375 to 0.09375
- x_kernel: bfloat16 [4, 8192], P(None, 'kv'), may hold values from -3 to 3
- bc_kernel: bfloat16 [4, 8192], P(None, 'kv'), may hold values from -3 to 3
- dt_bias: float32 [128], P('kv'), may hold values from -3 to 0.5
- decay_log: float32 [128], P('kv'), may hold values from -3 to 1.5
- skip_scale: float32 [128], P('kv'), may hold values from 0.5 to 1.5
- output_gain: bfloat16 [8192], P('kv'), may hold values from 0.099609375 to 1.8984375
- output_weight: bfloat16 [8192, 4096], P('kv'), may hold values from -0.25 to 0.25
- saved_states: float32 [32, 5, 128, 64, 128], P('tp', None, 'kv'), may hold values from -1.8 to 1.8
- x_history: bfloat16 [32, 7, 8192], P('tp', None, 'kv'), may hold values from -6 to 6
- bc_history: bfloat16 [32, 7, 8192], P('tp', None, 'kv'), may hold values from -6 to 6
- accepted: int32 [32], P('tp'), may hold values from 0 to 4
Outputs:
- mixed: bfloat16 [128, 4096], P('tp', 'kv')
- new_states: float32 [32, 5, 128, 64, 128], P('tp', None, 'kv')
- x_window: bfloat16 [32, 7, 8192], P('tp', None, 'kv')
- bc_window: bfloat16 [32, 7, 8192], P('tp', None, 'kv')
All inputs are finite; a program needn't handle non-finite values.
Results may differ from a plain program's by a relative error of at most 0.02.
Values may be sent and summed in bfloat16 or wider, within the bound.
A program may use at most 64 MiB of HBM per device.

v0:
```python
import jax
import jax.numpy as jnp
from jax import lax
from jax.sharding import Mesh
from jax.sharding import PartitionSpec as P

D = 4096
PROPS = 4
INNER = 8192
KV = ("kv_0", "kv_1", "kv_2")


EPSILON = 1e-05


def sent_to_all(value, axis):
    size = lax.axis_size(axis)
    return lax.all_to_all(
        jnp.broadcast_to(value[None], (size, *value.shape)), axis, 0, 0, tiled=True
    )


def over_copies(value, axis):
    return sent_to_all(value, axis).sum(axis=0)


def cut_along(value, dim, size):
    lengths = value.shape
    blocks = value.reshape(*lengths[:dim], size, lengths[dim] // size, *lengths[dim + 1 :])
    return jnp.moveaxis(blocks, dim, 0)


def sent_and_summed(value, axis, dim):
    blocks = cut_along(value, dim, lax.axis_size(axis))
    arrived = lax.all_to_all(blocks, axis, split_axis=0, concat_axis=0, tiled=True)
    return arrived.astype(jnp.float32).sum(axis=0)


def partner_2(block, axis, stride):
    count = lax.axis_size(axis)
    route = []
    for low in range(count):
        high = low | 1 << stride
        if high != low and high < count:
            route += [(low, high), (high, low)]
    return lax.ppermute(block, axis, route)


def one_axis_at_a_time(value, axes):
    far, near = axes
    nearer = over_copies(value, near)
    return over_copies(nearer, far)


def sent_and_summed_2(value, axis, dim):
    blocks = cut_along(value, dim, lax.axis_size(axis))
    arrived = lax.all_to_all(blocks, axis, split_axis=0, concat_axis=0, tiled=True)
    return arrived.sum(axis=0)


def summed_rows(value, axes, dim):
    far, near = axes
    own = sent_and_summed_2(cut_along(value, dim, lax.axis_size(far)), near, dim + 1)
    return jnp.sum(lax.all_to_all(own, far, 0, 0, tiled=True), axis=0)


def take_window(history, accepted, fresh_rows):
    history_len = history.shape[1] - fresh_rows.shape[1]
    indices = accepted[:, None] + jnp.arange(history_len, dtype=jnp.int32)[None, :]
    kept_rows = jnp.take_along_axis(history, indices[:, :, None], axis=1)
    return jnp.concatenate([kept_rows, fresh_rows], axis=1)


def conv_silu(window, kernel):
    length = window.shape[1] - kernel.shape[0] + 1
    running = window[:, 0:length].astype(jnp.float32) * kernel[0].astype(jnp.float32)
    for offset in range(1, kernel.shape[0]):
        running = running + window[:, offset : offset + length].astype(jnp.float32) * kernel[
            offset
        ].astype(jnp.float32)
    return jax.nn.silu(running)


def ssd_block(x_conv, step_size, decay_rate, b_terms, c_terms, first_state, skip_scale):
    cumulated = jnp.cumsum(-decay_rate * step_size, axis=1)
    length = x_conv.shape[1]
    indices = jnp.arange(length)
    causal = indices[:, None] >= indices[None, :]
    gaps = cumulated[:, :, None, :] - cumulated[:, None, :, :]
    weights = jnp.exp(jnp.where(causal[None, :, :, None], gaps, -jnp.inf))
    inputs = x_conv * step_size[..., None]
    outer_prod = jnp.einsum("srhp,srhn->srhpn", inputs, b_terms)
    states = jnp.exp(cumulated)[..., None, None] * first_state[:, None] + jnp.einsum(
        "strh,srhpn->sthpn", weights, outer_prod
    )
    output = jnp.einsum("sthn,sthpn->sthp", c_terms, states) + skip_scale[:, None] * x_conv
    return (output, states)


def local(
    hidden,
    input_gain,
    x_weight,
    z_weight,
    bc_weight,
    dt_weight,
    x_kernel,
    bc_kernel,
    dt_bias,
    decay_log,
    skip_scale,
    output_gain,
    output_weight,
    saved_states,
    x_history,
    bc_history,
    accepted,
):
    heads_here = dt_bias.shape[0]
    head_size = x_weight.shape[1] // heads_here
    state_size = saved_states.shape[4]
    seqs_here = accepted.shape[0]
    rows_here = hidden.shape[0] // lax.axis_size("tp")
    inner_here = x_weight.shape[1]
    bc_here = bc_weight.shape[1]
    widened = hidden.astype(jnp.float32)
    squares = over_copies(jnp.sum(widened * widened, axis=1), "tp")
    normed = (
        widened * lax.rsqrt(squares[:, None] / D + EPSILON) * input_gain.astype(jnp.float32)
    ).astype(jnp.bfloat16)
    weights = jnp.concatenate([x_weight, z_weight, bc_weight, dt_weight], axis=1)
    product = jnp.dot(normed, weights, preferred_element_type=jnp.float32)
    projected = sent_and_summed(
        lax.optimization_barrier(product.astype(jnp.bfloat16))
        .astype(jnp.float32)
        .astype(jnp.bfloat16),
        "tp",
        0,
    ).astype(jnp.bfloat16)
    x_fresh = projected[:, :inner_here]
    z_fresh = projected[:, inner_here : 2 * inner_here]
    bc_fresh = projected[:, 2 * inner_here : 2 * inner_here + bc_here]
    dt_fresh = projected[:, 2 * inner_here + bc_here :]
    x_window = take_window(x_history, accepted, x_fresh.reshape(seqs_here, PROPS, inner_here))
    bc_window = take_window(bc_history, accepted, bc_fresh.reshape(seqs_here, PROPS, bc_here))
    x_conv = conv_silu(x_window, x_kernel).reshape(seqs_here, PROPS, heads_here, head_size)
    bc_conv = conv_silu(bc_window, bc_kernel)
    spread = max(4 // heads_here, 1)
    position = lax.axis_index(KV)
    for level in range(spread.bit_length() - 1):
        partner = partner_2(bc_conv, KV, level)
        low_half = position // 2**level % 2 == 0
        bc_conv = jnp.where(
            low_half,
            jnp.concatenate([bc_conv, partner], axis=2),
            jnp.concatenate([partner, bc_conv], axis=2),
        )
    groups_here = bc_conv.shape[2] // (2 * state_size)
    paired = bc_conv.reshape(seqs_here, PROPS, groups_here, 2, state_size)
    per_group = heads_here // groups_here
    b_terms = jnp.repeat(paired[:, :, :, 0], per_group, axis=2)
    c_terms = jnp.repeat(paired[:, :, :, 1], per_group, axis=2)
    step_size = jax.nn.softplus(
        dt_fresh.astype(jnp.float32).reshape(seqs_here, PROPS, heads_here) + dt_bias
    )
    first_state = jnp.take_along_axis(saved_states, accepted[:, None, None, None, None], axis=1)[
        :, 0
    ]
    output, states = ssd_block(
        x_conv, step_size, jnp.exp(decay_log), b_terms, c_terms, first_state, skip_scale
    )
    new_states = jnp.concatenate([first_state[:, None], states], axis=1)
    gate_values = z_fresh.astype(jnp.float32).reshape(seqs_here, PROPS, heads_here, head_size)
    gated = (output * jax.nn.silu(gate_values)).reshape(rows_here, inner_here)
    square_sum = jnp.sum(gated * gated, axis=1)
    scaled = (gated * output_gain.astype(jnp.float32)).astype(jnp.bfloat16)
    partial_value = jnp.dot(scaled, output_weight, preferred_element_type=jnp.float32)
    total_squares = one_axis_at_a_time(square_sum, (("kv_0", "kv_1"), "kv_2"))
    summed = summed_rows(partial_value, (("kv_0", "kv_1"), "kv_2"), 1)
    mixed = (lax.rsqrt(total_squares / INNER + EPSILON)[:, None] * summed).astype(jnp.bfloat16)
    return (mixed, new_states, x_window, bc_window)


def solution(mesh):
    split = Mesh(mesh.devices.reshape(8, 8, 2, mesh.shape["tp"]), ("kv_0", "kv_1", "kv_2", "tp"))
    return jax.shard_map(
        local,
        mesh=split,
        in_specs=(
            P(None, "tp"),
            P("tp"),
            P("tp", KV),
            P("tp", KV),
            P("tp", KV),
            P("tp", KV),
            P(None, KV),
            P(None, KV),
            P(KV),
            P(KV),
            P(KV),
            P(KV),
            P(KV, None),
            P("tp", None, KV, None, None),
            P("tp", None, KV),
            P("tp", None, KV),
            P("tp"),
        ),
        out_specs=(
            P("tp", KV),
            P("tp", None, KV, None, None),
            P("tp", None, KV),
            P("tp", None, KV),
        ),
        check_vma=False,
    )
```

profile of v0, /device:TPU:1, one launch (start us, length us, event | category | flops | bytes accessed | tf_op | source)
XLA Modules:
  0.0 101.7 jit_solution(16168655335332894303)
XLA Ops:
  0.7 1.2 %fusion.4 = f32[128]{0:T(128)S(1)} fusion(bf16[128,1024]{1,0:T(8,128)(2,1)} %param.19), kind=kLoop, calls=%fused_computation.13 | loop fusion | flops 393088 | bytes 262656 | tf_op jit(solution)/shard_map/reduce_sum | solution.py:127
  2.5 4.8 %all-to-all-start = ((f32[4,1,128]{2,1,0:T(1,128)}), f32[4,1,128]{2,1,0:T(1,128)S(1)}, u32[]{:S(2)}, u32[]{:S(2)}) async-start(f32[4,1,128]{2,1,0:T(1,128)} %broadcast_in_dim.34), calls=%async_computation | async-start | bytes 4096 | tf_op jit(solution)/shard_map/all_to_all | solution.py:18
  10.2 0.8 bitcast_convert_fusion.3
  11.1 1.5 %gather_fusion.2 = bf16[24,64]{1,0:T(8,128)(2,1)S(1)} fusion(bf16[8,7,64]{2,0,1:T(8,128)(2,1)} %param.33, s32[24]{0:T(128)S(1)} %reshape.409), kind=kCustom, calls=%fused_computation.1.clone | custom fusion | bytes 6336 | tf_op jit(solution)/shard_map/jit(take_along_axis)/gather | solution.py:70
  12.6 1.5 %gather_fusion.1 = bf16[24,64]{1,0:T(8,128)(2,1)S(1)} fusion(bf16[8,7,64]{2,0,1:T(8,128)(2,1)} %param.34, s32[24]{0:T(128)S(1)} %reshape.409), kind=kCustom, calls=%fused_computation.clone | custom fusion | bytes 6336 | tf_op jit(solution)/shard_map/jit(take_along_axis)/gather | solution.py:70
  14.9 0.8 bitcast_convert_fusion.7
  15.7 0.7 convert_element_type.138
  16.4 1.5 %convolution_convert_fusion = bf16[128,193]{0,1:T(8,128)(2,1)S(1)} fusion(bf16[1024,1]{0,1:T(2,128)(2,1)} %param.24, bf16[1024,64]{0,1:T(8,128)(2,1)} %param.23, bf16[1024,64]{0,1:T(8,128)(2,1)} %param.22, bf16[1024,64]{0,1:T(8,128)(2,1)} %param.21, bf16[128,1024]{1,0:T(8,128)(2,1)} %param.19, f32[1024]{0:T(1024)S(1)} %convert_element_type.138, ...), kind=kOutput, calls=%fused_computation.7 | convolution fusion | flops 52723840 | bytes 711424 | tf_op jit(solution)/shard_map/dot_general | solution.py:132
  17.9 0.7 copy.102
  18.7 4.2 %all-to-all-start.1 = ((bf16[4,32,193]{2,1,0:T(8,128)(2,1)}), bf16[4,32,193]{2,1,0:T(8,128)(2,1)S(1)}, u32[]{:S(2)}, u32[]{:S(2)}) async-start(bf16[4,32,193]{2,1,0:T(8,128)(2,1)} %bitcast.2), calls=%async_computation.1 | async-start | bytes 131072 | tf_op jit(solution)/shard_map/all_to_all | solution.py:35
  25.4 2.0 %all-to-all-done.1 = bf16[4,32,193]{2,1,0:T(8,128)(2,1)S(1)} async-done(((bf16[4,32,193]{2,1,0:T(8,128)(2,1)}), bf16[4,32,193]{2,1,0:T(8,128)(2,1)S(1)}, u32[]{:S(2)}, u32[]{:S(2)}) %all-to-all-start.1) | async-done | bytes 49440 | tf_op jit(solution)/shard_map/all_to_all | solution.py:35
  27.8 8.8 %collective-permute-start = (f32[8,4,64]{2,1,0:T(4,128)S(1)}, f32[8,4,64]{2,1,0:T(4,128)S(1)}, u32[]{:S(2)}, u32[]{:S(2)}) collective-permute-start(f32[8,4,64]{2,1,0:T(4,128)S(1)} %divide_multiply_fusion.1), channel_id=1, source_target_pairs={{0,4},{4,0},{8,12},{12,8},{16,20},{20,16},{24,28},{28,24},{32,36},... | collective-permute-start | bytes 24584 | tf_op jit(solution)/shard_map/ppermute | solution.py:46
  36.7 0.8 collective-permute-done
  37.5 1.9 %collective-permute-start.1 = (f32[8,4,128]{2,1,0:T(4,128)S(1)}, f32[8,4,128]{2,1,0:T(4,128)S(1)}, u32[]{:S(2)}, u32[]{:S(2)}) collective-permute-start(f32[8,4,128]{2,1,0:T(4,128)S(1)} %maximum_select_fusion.1), channel_id=1, source_target_pairs={{0,8},{8,0},{4,12},{12,4},{16,24},{24,16},{20,28},{28,20},{32,40},... | collective-permute-start | bytes 49160 | tf_op jit(solution)/shard_map/ppermute | solution.py:46
  39.9 2.2 %collective-permute-done.1 = f32[8,4,128]{2,1,0:T(4,128)S(1)} collective-permute-done((f32[8,4,128]{2,1,0:T(4,128)S(1)}, f32[8,4,128]{2,1,0:T(4,128)S(1)}, u32[]{:S(2)}, u32[]{:S(2)}) %collective-permute-start.1) | collective-permute-done | bytes 16416 | tf_op jit(solution)/shard_map/ppermute | solution.py:46
  42.1 1.0 fusion
  43.1 1.0 copy-done.3
  44.6 4.8 %all_to_all.33 = f32[2,1,32]{2,1,0:T(1,128)S(1)} all-to-all(f32[2,1,32]{2,1,0:T(1,128)S(1)} %broadcast_in_dim.44), channel_id=1, replica_groups=mesh['kv_0'=8,'kv_1'=8,'kv_2'=2,'tp'=4] {'kv_2'}, dimensions={0} | all-to-all | bytes 512 | tf_op jit(solution)/shard_map/all_to_all | solution.py:18
  49.5 1.1 %convolution_bitcast_fusion = f32[64,32,64]{2,1,0:T(8,128)S(1)} fusion(bf16[32,64,1]{1,0,2:T(8,128)(2,1)S(1)} %bitcast.99, bf16[64,64,64]{2,1,0:T(8,128)(2,1)S(1)} %bitcast.89), kind=kOutput, calls=%fused_computation.4 | convolution fusion | flops 16777216 | bytes 1052672 | tf_op jit(solution)/shard_map/dot_general | solution.py:177
  51.3 0.7 reshape.422
  52.0 4.1 %all_to_all.34 = f32[2,1,65536]{2,1,0:T(1,128)S(1)} all-to-all(f32[2,1,65536]{2,1,0:T(1,128)S(1)} %reshape.422), channel_id=1, replica_groups=mesh['kv_0'=8,'kv_1'=8,'kv_2'=2,'tp'=4] {'kv_2'}, dimensions={0} | all-to-all | bytes 1048576 | tf_op jit(solution)/shard_map/all_to_all | solution.py:57
  56.7 12.1 %all-to-all-start.3 = ((f32[64,1,32]{2,1,0:T(1,128)}), f32[64,1,32]{2,1,0:T(1,128)S(1)}, u32[]{:S(2)}, u32[]{:S(2)}) async-start(f32[64,1,32]{2,1,0:T(1,128)} %broadcast_in_dim.45), calls=%async_computation.3 | async-start | bytes 65536 | tf_op jit(solution)/shard_map/all_to_all | solution.py:18
  69.3 2.3 %reduce.9 = f32[2,65536]{1,0:T(2,128)S(1)} reduce(f32[2,1,65536]{2,1,0:T(1,128)S(1)} %all_to_all.34, f32[]{:T(128)} %broadcast.283), dimensions={1}, to_apply=%all_to_all.25.reduce_sub_computation | reduce | bytes 1048580 | tf_op jit(solution)/shard_map/all_to_all | solution.py:57
  72.4 0.9 copy.112
  73.3 1.2 %reshape.424 = f32[64,1,1024]{2,1,0:T(1,128)} reshape(f32[64,32,32]{2,1,0:T(8,128)S(1)} %copy.112) | data formatting | bytes 524288
  74.5 5.2 %all-to-all-done.3 = f32[64,1,32]{2,1,0:T(1,128)S(1)} async-done(((f32[64,1,32]{2,1,0:T(1,128)}), f32[64,1,32]{2,1,0:T(1,128)S(1)}, u32[]{:S(2)}, u32[]{:S(2)}) %all-to-all-start.3) | async-done | bytes 8224 | tf_op jit(solution)/shard_map/all_to_all | solution.py:18
  79.6 7.0 %all-to-all-start.5 = ((f32[64,1,1024]{2,1,0:T(1,128)}), f32[64,1,1024]{2,1,0:T(1,128)S(1)}, u32[]{:S(2)}, u32[]{:S(2)}) async-start(f32[64,1,1024]{2,1,0:T(1,128)} %reshape.424), calls=%async_computation.5 | async-start | bytes 524288 | tf_op jit(solution)/shard_map/all_to_all | solution.py:64
  88.2 1.7 %pad_maximum_fusion = f32[8,5,1,64,128]{4,1,3,0,2:T(8,128)S(1)} fusion(f32[8,4,1,64,128]{4,1,3,0,2:T(4,128)} %copy-done.3, f32[8,1,1,64,128]{4,1,3,0,2:T(1,128)S(1)} %broadcast_select_fusion), kind=kLoop, calls=%fused_computation.3 | loop fusion | flops 327680 | bytes 2621440 | tf_op jit(solution)/shard_map/concatenate | solution.py:172
  89.8 1.3 %copy.113 = f32[8,5,1,64,128]{4,3,2,1,0:T(8,128)} copy(f32[8,5,1,64,128]{4,1,3,0,2:T(8,128)S(1)} %pad_maximum_fusion) | data formatting | bytes 2621440
  91.2 8.1 %all-to-all-done.5 = f32[64,1,1024]{2,1,0:T(1,128)S(1)} async-done(((f32[64,1,1024]{2,1,0:T(1,128)}), f32[64,1,1024]{2,1,0:T(1,128)S(1)}, u32[]{:S(2)}, u32[]{:S(2)}) %all-to-all-start.5) | async-done | bytes 262176 | tf_op jit(solution)/shard_map/all_to_all | solution.py:64
  99.3 1.3 %reduce.10 = f32[64,1024]{1,0:T(8,128)S(1)} reduce(f32[64,1,1024]{2,1,0:T(1,128)S(1)} %all-to-all-done.5, f32[]{:T(128)} %broadcast.283), dimensions={1}, to_apply=%all_to_all.26.reduce_sub_computation | reduce | bytes 524292 | tf_op jit(solution)/shard_map/all_to_all | solution.py:64
  101.0 0.7 multiply_convert_fusion
  (67 shorter events, 11.0 us)
Async XLA Ops:
  0.6 13.5 %copy-start = (f32[8,5,1,64,128]{4,3,2,1,0:T(8,128)S(1)}, f32[8,5,1,64,128]{4,3,2,1,0:T(8,128)}, u32[]{:S(2)}) copy-start(f32[8,5,1,64,128]{4,3,2,1,0:T(8,128)} %param.32) | copy-start | bytes 3932164
  0.6 24.3 %copy-start.5 = (bf16[64]{0:T(256)(128)(2,1)S(1)}, bf16[64]{0:T(256)(128)(2,1)}, u32[]{:S(2)}) copy-start(bf16[64]{0:T(256)(128)(2,1)} %param.30) | copy-start | bytes 388
  0.7 24.3 %copy-start.4 = (bf16[64,4096]{1,0:T(8,128)(2,1)S(1)}, bf16[64,4096]{1,0:T(8,128)(2,1)}, u32[]{:S(2)}) copy-start(bf16[64,4096]{1,0:T(8,128)(2,1)} %param.31) | copy-start | bytes 1572868
  2.5 13.9 %all-to-all-start = ((f32[4,1,128]{2,1,0:T(1,128)}), f32[4,1,128]{2,1,0:T(1,128)S(1)}, u32[]{:S(2)}, u32[]{:S(2)}) async-start(f32[4,1,128]{2,1,0:T(1,128)} %broadcast_in_dim.34), calls=%async_computation | async-start | bytes 4096 | tf_op jit(solution)/shard_map/all_to_all | solution.py:18
  14.7 10.2 %copy-start.1 = (f32[8,64,128]{2,1,0:T(8,128)}, f32[8,64,128]{2,1,0:T(8,128)S(1)}, u32[]{:S(2)}) copy-start(f32[8,64,128]{2,1,0:T(8,128)S(1)} %gather_fusion) | copy-start | bytes 786436
  18.7 8.7 %all-to-all-start.1 = ((bf16[4,32,193]{2,1,0:T(8,128)(2,1)}), bf16[4,32,193]{2,1,0:T(8,128)(2,1)S(1)}, u32[]{:S(2)}, u32[]{:S(2)}) async-start(bf16[4,32,193]{2,1,0:T(8,128)(2,1)} %bitcast.2), calls=%async_computation.1 | async-start | bytes 131072 | tf_op jit(solution)/shard_map/all_to_all | solution.py:35
  27.8 9.6 %collective-permute-start = (f32[8,4,64]{2,1,0:T(4,128)S(1)}, f32[8,4,64]{2,1,0:T(4,128)S(1)}, u32[]{:S(2)}, u32[]{:S(2)}) collective-permute-start(f32[8,4,64]{2,1,0:T(4,128)S(1)} %divide_multiply_fusion.1), channel_id=1, source_target_pairs={{0,4},{4,0},{8,12},{12,8},{16,20},{20,16},{24,28},{28,24},{32,36},... | collective-permute-start | bytes 24584 | tf_op jit(solution)/shard_map/ppermute | solution.py:46
  37.5 4.5 %collective-permute-start.1 = (f32[8,4,128]{2,1,0:T(4,128)S(1)}, f32[8,4,128]{2,1,0:T(4,128)S(1)}, u32[]{:S(2)}, u32[]{:S(2)}) collective-permute-start(f32[8,4,128]{2,1,0:T(4,128)S(1)} %maximum_select_fusion.1), channel_id=1, source_target_pairs={{0,8},{8,0},{4,12},{12,4},{16,24},{24,16},{20,28},{28,20},{32,40},... | collective-permute-start | bytes 49160 | tf_op jit(solution)/shard_map/ppermute | solution.py:46
  43.1 1.0 copy-start.3
  56.7 22.9 %all-to-all-start.3 = ((f32[64,1,32]{2,1,0:T(1,128)}), f32[64,1,32]{2,1,0:T(1,128)S(1)}, u32[]{:S(2)}, u32[]{:S(2)}) async-start(f32[64,1,32]{2,1,0:T(1,128)} %broadcast_in_dim.45), calls=%async_computation.3 | async-start | bytes 65536 | tf_op jit(solution)/shard_map/all_to_all | solution.py:18
  72.4 14.3 %copy-start.2 = (f32[8,64,128]{2,1,0:T(8,128)S(1)}, f32[8,64,128]{2,1,0:T(8,128)}, u32[]{:S(2)}) copy-start(f32[8,64,128]{2,1,0:T(8,128)} %copy-done.1) | copy-start | bytes 786436
  79.6 19.6 %all-to-all-start.5 = ((f32[64,1,1024]{2,1,0:T(1,128)}), f32[64,1,1024]{2,1,0:T(1,128)S(1)}, u32[]{:S(2)}, u32[]{:S(2)}) async-start(f32[64,1,1024]{2,1,0:T(1,128)} %reshape.424), calls=%async_computation.5 | async-start | bytes 524288 | tf_op jit(solution)/shard_map/all_to_all | solution.py:64
where the time goes:
time: 104 us; the launch traced here: 102 us
  starting transfers between devices  38.8 us (37%)
  waiting for transfers between devices  18.1 us (17%)
  local copies, waits for them, and re-layouts  15.2 us (15%)
  other arithmetic  13.7 us (13%)
  blocking collectives  8.97 us (9%)
  matrix products  3.9 us (4%)
  between operations  2.93 us (3%)
    all_to_all x2, starting transfers between devices, sent_to_all(): lax.all_to_all(jnp.broadcast_to(value[None], (size, *value.shape)), axis,...  16.9 us
    ppermute x2, starting transfers between devices, partner_2(): return lax.ppermute(block, axis, route)  10.7 us
    all_to_all x1, waiting for transfers between devices, summed_rows(): return jnp.sum(lax.all_to_all(own, far, 0, 0, tiled=True), axis=0)  8.07 us
    all_to_all x1, starting transfers between devices, summed_rows(): return jnp.sum(lax.all_to_all(own, far, 0, 0, tiled=True), axis=0)  6.97 us
    unnamed x20, local copies, waits for them, and re-layouts  6.3 us
    all_to_all x2, waiting for transfers between devices, sent_to_all(): lax.all_to_all(jnp.broadcast_to(value[None], (size, *value.shape)), axis,...  5.17 us
    all_to_all x1, blocking collectives, sent_to_all(): lax.all_to_all(jnp.broadcast_to(value[None], (size, *value.shape)), axis,...  4.85 us
    all_to_all x1, starting transfers between devices, sent_and_summed(): lax.all_to_all(blocks, axis, split_axis=0, concat_axis=0, tiled=True)  4.24 us
  transfers between devices with their start and end apart: 6, of which 5 were waited for; matrix products, arithmetic and copies ran while one was open for 20% of the time, Pallas kernels for 0%

commit v1 on v0

v1 whole, which is shorter than its diff:
```python
import jax
import jax.numpy as jnp
from jax import lax
from jax.experimental import pallas as pl
from jax.experimental.pallas import tpu as pltpu
from jax.sharding import PartitionSpec as P

D = 4096
INNER = 8192
EPSILON = 1e-05
MESH = pl.DeviceIdType.MESH
F32 = jnp.float32
BF16 = jnp.bfloat16
SIDE = 8
CHIPS = 64
STEPS = sorted(
    ((dz, dy) for dz in range(SIDE) for dy in range(SIDE) if dz or dy),
    key=lambda p: -(min(p[0], SIDE - p[0]) + min(p[1], SIDE - p[1])),
)


def iota(shape, dim):
    return lax.broadcasted_iota(jnp.int32, shape, dim)


def silu(v):
    return v / (1.0 + jnp.exp(-v))


def softplus(v):
    return jnp.maximum(v, 0.0) + jnp.log1p(jnp.exp(-jnp.abs(v)))


def wait_for(ref, sem):
    pltpu.make_async_copy(ref, ref, sem).wait()


def transpose_blocks(rows):
    lane = iota((8, 128), 1)
    low = lane < 64
    even = lax.rem(lane, 64) < 32
    half = [None] * 4
    for g in range(2):
        near, far = rows[g], rows[g + 2]
        half[g] = jnp.where(low, near, pltpu.roll(far, 64, 1))
        half[g + 2] = jnp.where(low, pltpu.roll(near, 64, 1), far)
    out = []
    for g in (0, 2):
        near, far = half[g], half[g + 1]
        out.append(jnp.where(even, near, pltpu.roll(far, 32, 1)))
        out.append(jnp.where(even, pltpu.roll(near, 96, 1), far))
    return out


def mixer(
    hidden, gain, xw, zw, bcw, dtw, xk, bck, ogain, ow, saved, xh, bch,
    accepted_h, dt_bias, decay_log, skip,
    mixed, states, xwin, bcwin,
    hidden_v, gain_v, wt_v, dt_v, xk_v, bck_v, ogain_v, ow_v, saved_v, xh_v, bch_v,
    hg_v, prod_v, fb_v,
    sa, sb, ra, rb, hs, hr,
    pb, pr, ob, ro, qs, qr, qp, rq, ms,
    accepted, load, sa_s, sb_s, hs_s, ra_s, rb_s, hr_s, pb_s, pr_s, qs_s, qr_s, ob_s, ro_s, qp_s, rq_s, ready,
):
    kv = lax.axis_index("kv")
    tp = lax.axis_index("tp")
    core = lax.rem(kv, 2)
    chip = lax.div(kv, 2)
    y = lax.rem(chip, SIDE)
    z = lax.div(chip, SIDE)
    member = lax.rem(kv, 4)
    base = kv - member

    loads = []

    def fetch(src, dst):
        copy = pltpu.make_async_copy(src, dst, load.at[len(loads)])
        copy.start()
        loads.append(copy)
        return copy

    l_hidden = fetch(hidden, hidden_v)
    l_gain = fetch(gain, gain_v)
    l_dt = fetch(dtw, dt_v)
    l_w = [
        fetch(xw, wt_v.at[pl.ds(0, 64)]),
        fetch(zw, wt_v.at[pl.ds(64, 64)]),
        fetch(bcw, wt_v.at[pl.ds(128, 64)]),
    ]

    barrier = pltpu.get_barrier_semaphore()

    def greet(k, t):
        pl.semaphore_signal(barrier, inc=1, device_id=(k, t), device_id_type=MESH)

    for d in range(1, SIDE):
        greet((lax.rem(z + d, SIDE) * SIDE + y) * 2 + core, tp)
        greet((z * SIDE + lax.rem(y + d, SIDE)) * 2 + core, tp)
    for dm in range(4):
        for dt in range(4):
            if dm or dt:
                greet(base + lax.rem(member + dm, 4), lax.rem(tp + dt, 4))

    l_hist = [fetch(accepted_h, accepted), fetch(xh, xh_v), fetch(bch, bch_v), fetch(xk, xk_v), fetch(bck, bck_v)]
    l_saved = fetch(saved, saved_v)
    l_ow = fetch(ow, ow_v)
    l_ogain = fetch(ogain, ogain_v)

    wt_v[pl.ds(192, 64), :] = jnp.zeros((64, 1024), BF16)
    l_gain.wait()
    l_hidden.wait()
    l_dt.wait()
    gains = gain_v[...].astype(F32)
    gain_row = jnp.concatenate([gains[j : j + 1] for j in range(8)], axis=1)
    dt_row = dt_v[...].astype(F32)
    squares, dts = [], []
    for i in range(4):
        wide = hidden_v[pl.ds(32 * i, 32), :].astype(F32)
        squares.append(jnp.sum(wide * wide, axis=1, keepdims=True))
        gained = (wide * gain_row).astype(BF16)
        hg_v[pl.ds(32 * i, 32), :] = gained
        dts.append(jnp.sum(gained.astype(F32) * dt_row, axis=1, keepdims=True))
    for copy in l_w:
        copy.wait()
    product = lax.dot_general(
        hg_v[...], wt_v[...], (((1,), (1,)), ((), ())), preferred_element_type=F32
    )
    lane32 = iota((32, 128), 1)
    prod_v[0] = product[:, 0:128]
    for i in range(4):
        high = squares[i].astype(BF16).astype(F32)
        tail = product[32 * i : 32 * i + 32, 128:256]
        tail = jnp.where(lane32 == 64, dts[i], tail)
        tail = jnp.where(lane32 == 65, high, tail)
        tail = jnp.where(lane32 == 66, squares[i] - high, tail)
        prod_v[1, pl.ds(32 * i, 32), :] = tail
    for i in range(4):
        for part, out in ((0, sa), (1, sb)):
            rows = [prod_v[part, pl.ds(32 * i + t, 8, stride=4), :] for t in range(4)]
            out[i] = jnp.concatenate(rows, axis=0).astype(BF16)

    for copy in l_hist:
        copy.wait()
    seq = iota((8, 64), 0)
    acc = jnp.zeros((8, 64), jnp.int32)
    for s in range(8):
        acc = jnp.where(seq == s, accepted[s], acc)

    def kept(history):
        wide = [history[i].astype(F32) for i in range(7)]
        out = []
        for j in range(3):
            row = wide[j]
            for k in range(1, 5):
                row = jnp.where(acc == k, wide[j + k], row)
            out.append(row)
        return out

    x_kept = kept(xh_v)
    bc_kept = kept(bch_v)
    packed = jnp.concatenate([*bc_kept, bck_v[...].astype(F32), jnp.zeros((4, 64), F32)], axis=0)
    packed = jnp.concatenate([packed, jnp.zeros((32, 64), F32)], axis=1).astype(BF16)
    hs[...] = packed
    hr[member] = packed
    rb[4 * member] = sb[tp]

    pl.semaphore_wait(barrier, 29)
    for d in range(1, SIDE):
        pl.semaphore_signal(
            ready,
            inc=1,
            device_id=((lax.rem(z + d, SIDE) * SIDE + y) * 2 + core, tp),
            device_id_type=MESH,
        )

    def send(src, dst, send_sem, recv_sem, k, t):
        copy = pltpu.make_async_remote_copy(
            src_ref=src,
            dst_ref=dst,
            send_sem=send_sem,
            recv_sem=recv_sem,
            device_id=(k, t),
            device_id_type=MESH,
        )
        copy.start()
        return copy

    for dt in (2, 1, 3, 0):
        to_t = lax.rem(tp + dt, 4)
        for dm in (2, 3, 1, 0):
            to_k = base + lax.rem(member + dm, 4)
            if dm or dt:
                send(sb.at[to_t], rb.at[4 * member + (4 - dt) % 4], sb_s, rb_s, to_k, to_t)
        if dt:
            send(sa.at[to_t], ra.at[4 - dt], sa_s, ra_s, kv, to_t)
    for dm in (2, 3, 1):
        send(hs, hr.at[member], hs_s, hr_s, base + lax.rem(member + dm, 4), tp)

    l_saved.wait()
    for s in range(8):
        first = saved_v[s, accepted[s]]
        states[s, 0] = first
        fb_v[pl.ds(64 * s, 64), :] = first.astype(BF16)
    l_ogain.wait()
    l_ow.wait()

    wait_for(ra.at[pl.ds(1, 3)], ra_s)
    wait_for(rb.at[pl.ds(0, 15)], rb_s)
    wait_for(hr.at[pl.ds(0, 3)], hr_s)

    def total(blocks):
        out = blocks[0].astype(F32)
        for block in blocks[1:]:
            out = out + block.astype(F32)
        return out

    own = total([rb[4 * member + i] for i in range(4)])
    square_sum = own[:, 65:66] + own[:, 66:67]
    scale = jnp.broadcast_to(lax.rsqrt(square_sum / D + EPSILON), (32, 128))
    xz = (total([sa[tp]] + [ra[i] for i in range(1, 4)]) * scale).astype(BF16).astype(F32)
    dt_fresh = (own * scale).astype(BF16).astype(F32)[:, 64:65]
    fresh = [
        (total([rb[4 * m + i] for i in range(4)]) * scale).astype(BF16).astype(F32)[:, 0:64]
        for m in range(4)
    ]
    stored = [hr[m].astype(F32)[:, 0:64] for m in range(4)]

    def conv(rows, taps):
        out = []
        for t in range(4):
            value = rows[t] * taps[0:1]
            for j in range(1, 4):
                value = value + rows[t + j] * taps[j : j + 1]
            out.append(silu(value))
        return out

    def pieces(value):
        return [value[8 * t : 8 * t + 8] for t in range(4)]

    x_rows = x_kept + pieces(xz[:, 0:64])
    x_conv = conv(x_rows, xk_v[...].astype(F32))
    terms = []
    for low, high in ((0, 1), (2, 3)):
        new = pieces(jnp.concatenate([fresh[low], fresh[high]], axis=1))
        old = jnp.concatenate([stored[low], stored[high]], axis=1)
        taps = old[24:28]
        terms.append(conv(pieces(old)[:3] + new, taps))
    b_terms, c_terms = terms

    rate = jnp.exp(jnp.full((8, 128), decay_log[0], F32))
    steps = pieces(softplus(jnp.broadcast_to(dt_fresh, (32, 128)) + dt_bias[0]))
    cumulated = []
    for t in range(4):
        value = -rate * steps[t]
        cumulated.append(value if t == 0 else cumulated[-1] + value)

    reads = lax.dot_general(
        jnp.concatenate(c_terms, axis=0).astype(BF16),
        fb_v[...],
        (((1,), (1,)), ((), ())),
        preferred_element_type=F32,
    )
    which = lax.rem(iota((32, 128), 0), 8) - jnp.where(lane32 < 64, 0, 1)
    picked = jnp.where(which == 0, reads[:, 0:128], 0.0)
    for i in range(1, 4):
        picked = picked + jnp.where(which == 2 * i, reads[:, 128 * i : 128 * i + 128], 0.0)
    first_part = pieces(picked[:, 0:64] + picked[:, 64:128])

    gated = []
    z_rows = pieces(xz[:, 64:128])
    for t in range(4):
        value = jnp.exp(cumulated[t])[:, 0:64] * first_part[t] + skip[0] * x_conv[t]
        for r in range(t + 1):
            weight = jnp.exp(cumulated[t] - cumulated[r]) * steps[r] if r < t else steps[r]
            inner = jnp.sum(c_terms[t] * b_terms[r], axis=1, keepdims=True)
            value = value + weight[:, 0:64] * inner * x_conv[r]
        gated.append(value * silu(z_rows[t]))
    gated = jnp.concatenate(gated, axis=0)
    square_sum = jnp.sum(gated * gated, axis=1, keepdims=True)
    diagonal = iota((32, 128), 0) == lane32
    row = jnp.sum(jnp.where(diagonal, square_sum, 0.0), axis=0, keepdims=True)
    qs[...] = row
    partner = kv + 1 - 2 * core
    send(qs, qr, qs_s, qr_s, partner, tp)
    scaled = (gated * ogain_v[...].astype(F32)).astype(BF16)

    for k in range(4):
        for n in range(2 * k, 2 * k + 2):
            partial = jnp.dot(
                scaled, ow_v[:, 512 * n : 512 * n + 512], preferred_element_type=F32
            )
            for i in range(4):
                tile = partial[:, 128 * i : 128 * i + 128]
                blocks = transpose_blocks(pieces(tile))
                for b in range(4):
                    pb[b % 2, 2 * (4 * n + i) + b // 2] = blocks[b].astype(BF16)
        part = pl.ds(16 * k, 16)
        send(pb.at[1 - core, part], pr.at[part], pb_s.at[k], pr_s.at[k], partner, tp)

    wait_for(qr, qr_s)
    qp[...] = qs[...] + qr[...]
    pl.semaphore_wait(ready, SIDE - 1)

    def at(dz, dy):
        return lax.rem(z + dz, SIDE) * SIDE + lax.rem(y + dy, SIDE)

    for dz, dy in STEPS:
        send(qp, rq.at[dz * SIDE + dy], qp_s, rq_s, at(dz, dy) * 2 + core, tp)
    for k in range(4):
        part = pl.ds(16 * k, 16)
        wait_for(pr.at[part], pr_s.at[k])
        ob[part] = (pb[core, part].astype(F32) + pr[part].astype(F32)).astype(BF16)
    for dz, dy in STEPS:
        to = at(dz, dy)
        send(ob.at[to], ro.at[dz * SIDE + dy], ob_s, ro_s, to * 2 + core, tp)

    x_in = jnp.concatenate([x_conv[t] * steps[t][:, 0:64] for t in range(4)], axis=0)
    x_cols = jnp.transpose(jnp.concatenate([x_in, jnp.zeros((32, 64), F32)], axis=1))
    decays = [jnp.exp(-rate * steps[t]) for t in range(4)]
    for s in range(8):
        state = saved_v[s, accepted[s]]
        for t in range(4):
            i = 8 * t + s
            state = state * decays[t][s : s + 1] + x_cols[0:64, i : i + 1] * b_terms[t][s : s + 1]
            states[s, t + 1] = state
    for j in range(7):
        xwin[j] = x_rows[j].astype(BF16)
    bc_rows = bc_kept + pieces((own * scale).astype(BF16).astype(F32)[:, 0:64])
    for j in range(7):
        bcwin[j] = bc_rows[j].astype(BF16)

    wait_for(rq.at[pl.ds(1, CHIPS - 1)], rq_s)
    squares_row = qp[...] + jnp.sum(rq[pl.ds(1, CHIPS - 1)], axis=0)
    column = jnp.sum(jnp.where(diagonal, squares_row, 0.0), axis=1, keepdims=True)
    factor = lax.rsqrt(column / INNER + EPSILON)
    wait_for(ro.at[pl.ds(1, CHIPS - 1)], ro_s)
    summed = ob[chip].astype(F32) + jnp.sum(ro[pl.ds(1, CHIPS - 1)].astype(F32), axis=0)
    for t in range(4):
        shifted = pltpu.roll(summed, (128 - 32 * t) % 128, 1) if t else summed
        ms[pl.ds(t, 8, stride=4), :] = shifted * factor[8 * t : 8 * t + 8]
    mixed[...] = ms[:, 0:32].astype(BF16)

    wait_for(sa.at[pl.ds(0, 3)], sa_s)
    wait_for(rb.at[pl.ds(0, 15)], sb_s)
    wait_for(hr.at[pl.ds(0, 3)], hs_s)
    wait_for(qs, qs_s)
    for k in range(4):
        wait_for(pr.at[pl.ds(16 * k, 16)], pb_s.at[k])
    wait_for(rq.at[pl.ds(1, CHIPS - 1)], qp_s)
    wait_for(ro.at[pl.ds(1, CHIPS - 1)], ob_s)


def writer(mixed, states, xwin, bcwin, mixed_o, states_o, xwin_o, bcwin_o, sem):
    copies = [
        pltpu.make_async_copy(states.at[pl.ds(2 * i, 2)], states_o.at[pl.ds(2 * i, 2)], sem.at[i])
        for i in range(4)
    ]
    copies.append(pltpu.make_async_copy(mixed, mixed_o, sem.at[4]))
    copies.append(pltpu.make_async_copy(xwin, xwin_o, sem.at[5]))
    copies.append(pltpu.make_async_copy(bcwin, bcwin_o, sem.at[6]))
    for copy in copies:
        copy.start()
    for copy in copies:
        copy.wait()


def local(
    hidden, input_gain, x_weight, z_weight, bc_weight, dt_weight, x_kernel, bc_kernel,
    dt_bias, decay_log, skip_scale, output_gain, output_weight, saved_states, x_history,
    bc_history, accepted,
):
    shapes = [((32, 32), BF16), ((8, 5, 64, 128), F32), ((7, 8, 64), BF16), ((7, 8, 64), BF16)]
    hbm = pl.BlockSpec(memory_space=pltpu.HBM)
    vmem = pl.BlockSpec(memory_space=pltpu.VMEM)
    smem = pl.BlockSpec(memory_space=pltpu.SMEM)
    dma = pltpu.SemaphoreType.DMA
    scratch = [
        ((128, 1024), BF16), ((8, 128), BF16), ((256, 1024), BF16), ((1, 1024), BF16),
        ((4, 64), BF16), ((4, 64), BF16), ((1, 64), BF16), ((64, 4096), BF16),
        ((8, 5, 64, 128), F32), ((7, 8, 64), BF16), ((7, 8, 64), BF16),
        ((128, 1024), BF16), ((2, 128, 128), F32), ((512, 128), BF16),
        ((4, 32, 128), BF16), ((4, 32, 128), BF16), ((4, 32, 128), BF16), ((16, 32, 128), BF16),
        ((32, 128), BF16), ((4, 32, 128), BF16),
        ((2, 64, 8, 128), BF16), ((64, 8, 128), BF16), ((64, 8, 128), BF16), ((64, 8, 128), BF16),
        ((1, 128), F32), ((1, 128), F32), ((1, 128), F32), ((64, 1, 128), F32), ((32, 128), F32),
    ]
    args = [
        hidden, input_gain.reshape(8, 128), x_weight.T, z_weight.T, bc_weight.T, dt_weight.T,
        x_kernel, bc_kernel, output_gain.reshape(1, 64), output_weight,
        saved_states.reshape(8, 5, 64, 128), x_history.transpose(1, 0, 2),
        bc_history.transpose(1, 0, 2), accepted,
    ]
    args = [pltpu.with_memory_space_constraint(arg, pltpu.HBM) for arg in args]
    results = pl.pallas_call(
        mixer,
        name="mixer",
        out_shape=[pltpu.VMEM(shape, dtype) for shape, dtype in shapes],
        in_specs=[hbm] * len(args) + [smem] * 3,
        out_specs=[vmem] * 4,
        scratch_shapes=[pltpu.VMEM(shape, dtype) for shape, dtype in scratch]
        + [pltpu.SMEM((8,), jnp.int32), dma((20,))]
        + [dma(())] * 6
        + [dma((4,)), dma((4,))]
        + [dma(())] * 6
        + [pltpu.SemaphoreType.REGULAR],
        compiler_params=pltpu.CompilerParams(
            collective_id=0, has_side_effects=True, vmem_limit_bytes=24 << 20
        ),
    )(*args, dt_bias, decay_log, skip_scale)
    mixed, states, xwin, bcwin = pl.pallas_call(
        writer,
        name="writer",
        out_shape=[jax.ShapeDtypeStruct(shape, dtype) for shape, dtype in shapes],
        in_specs=[vmem] * 4,
        out_specs=[hbm] * 4,
        scratch_shapes=[dma((7,))],
        compiler_params=pltpu.CompilerParams(vmem_limit_bytes=8 << 20),
    )(*results)
    return (
        mixed,
        states.reshape(8, 5, 1, 64, 128),
        xwin.transpose(1, 0, 2),
        bcwin.transpose(1, 0, 2),
    )


def solution(mesh):
    return jax.shard_map(
        local,
        mesh=mesh,
        in_specs=(
            P(None, "tp"), P("tp"), P("tp", "kv"), P("tp", "kv"), P("tp", "kv"), P("tp", "kv"),
            P(None, "kv"), P(None, "kv"), P("kv"), P("kv"), P("kv"), P("kv"), P("kv", None),
            P("tp", None, "kv", None, None), P("tp", None, "kv"), P("tp", None, "kv"), P("tp"),
        ),
        out_specs=(
            P("tp", "kv"), P("tp", None, "kv", None, None), P("tp", None, "kv"), P("tp", None, "kv"),
        ),
        check_vma=False,
    )
```

time: 104 us -> 33.4 us (0.32); the launches traced: 102 us -> 33.2 us
  starting transfers between devices: 38.8 us -> 0 us
  Pallas kernels: 0 us -> 30.6 us
  waiting for transfers between devices: 18.1 us -> 0 us
  local copies, waits for them, and re-layouts: 15.2 us -> 0 us
  other arithmetic: 13.7 us -> 0 us
  blocking collectives: 8.97 us -> 0 us
  matrix products: 3.9 us -> 0 us
    pallas_call x0 -> x2, Pallas kernels: none -> 30.6 us  [the longest x1 29.5 us: local(): pl.pallas_call(mixer, name='mixer', out_shape=[pltpu.VMEM(shape, dtype) f...]
    all_to_all x4 -> x0, starting transfers between devices: 28.1 us -> none  [the longest x2 16.9 us: sent_to_all(): lax.all_to_all(jnp.broadcast_to(value[None], (size, *value.shape)), axis,...]
    all_to_all x4 -> x0, waiting for transfers between devices: 15.2 us -> none  [the longest x1 8.07 us: summed_rows(): return jnp.sum(lax.all_to_all(own, far, 0, 0, tiled=True), axis=0)]
    ppermute x2 -> x0, starting transfers between devices: 10.7 us -> none  [partner_2(): return lax.ppermute(block, axis, route)]
    all_to_all x2 -> x0, blocking collectives: 8.97 us -> none  [the longest x1 4.85 us: sent_to_all(): lax.all_to_all(jnp.broadcast_to(value[None], (size, *value.shape)), axis,...]
    unnamed x20 -> x0, local copies, waits for them, and re-layouts: 6.3 us -> none
    dot_general x4 -> x0, matrix products: 3.9 us -> none  [the longest x1 1.5 us: local(): product = jnp.dot(normed, weights, preferred_element_type=jnp.float32)]
    gather x7 -> x0, local copies, waits for them, and re-layouts: 3.77 us -> none  [the longest x6 3.19 us: take_window(): kept_rows = jnp.take_along_axis(history, indices[:, :, None], axis=1)]
  transfers between devices with their start and end apart: 6 -> 0, of which waited for: 5 -> 0; matrix products, arithmetic and copies ran while one was open for 20% -> 0% of each run, Pallas kernels for 0% -> 0%
where the time goes in v1:
time: 33.4 us; the launch traced here: 33.2 us
  Pallas kernels  30.6 us (92%)
  between operations  2.58 us (8%)
    pallas_call x1, Pallas kernels, local(): pl.pallas_call(mixer, name='mixer', out_shape=[pltpu.VMEM(shape, dtype) f...  29.5 us
    pallas_call x1, Pallas kernels, local(): pl.pallas_call(writer, name='writer', out_shape=[jax.ShapeDtypeStruct(sha...  1.12 us

profile of v1, /device:TPU:1, one launch (start us, length us, event | category | flops | bytes accessed | tf_op | source)
XLA Modules:
  0.0 33.2 jit_solution(7952337475941249766)
XLA Ops:
  2.6 29.5 %mixer.1 = (bf16[32,32]{1,0:T(8,128)(2,1)S(1)}, f32[8,5,64,128]{3,2,1,0:T(8,128)S(1)}, bf16[7,8,64]{2,1,0:T(8,128)(2,1)S(1)}, bf16[7,8,64]{2,1,0:T(8,128)(2,1)S(1)}) custom-call(bf16[128,1024]{1,0:T(8,128)(2,1)} %hidden.1, bf16[8,128]{1,0:T(8,128)(2,1)} %bitcast.21, bf16[64,1024]{1,0:T(8,128)(2,1)} %bitcast.15, bf16[64,1024]{1,0:T(8,128)(2,1)} %bitcast.16, ...), custom_call_target="tpu_custom_call" | custom-call | tf_op jit(solution)/shard_map/mixer/pallas_call | solution.py:394
  32.1 1.1 %writer.1 = (bf16[32,32]{1,0:T(8,128)(2,1)}, f32[8,5,64,128]{3,2,1,0:T(8,128)}, bf16[7,8,64]{2,1,0:T(8,128)(2,1)}, bf16[7,8,64]{2,1,0:T(8,128)(2,1)}) custom-call(bf16[32,32]{1,0:T(8,128)(2,1)S(1)} %get-tuple-element.12.mixed, f32[8,5,64,128]{3,2,1,0:T(8,128)S(1)} %get-tuple-element.13.states, bf16[7,8,64]{2,1,0:T(8,128)(2,1)S(1)} %get-tuple-element.14.xwin, ...), custom_call_target="tpu_custom_call" | custom-call | tf_op jit(solution)/shard_map/writer/pallas_call | solution.py:410

commit v2 on v1

--- a/solution.py
+++ b/solution.py
@@ -12,9 +12,10 @@
 F32 = jnp.float32
 BF16 = jnp.bfloat16
 SIDE = 8
-CHIPS = 64
-STEPS = sorted(
-    ((dz, dy) for dz in range(SIDE) for dy in range(SIDE) if dz or dy),
+FAR = (4, 3, 5, 2, 6, 1, 7, 0)
+CORNER = [(dz, dy) for dz in FAR[:3] for dy in FAR[:3]]
+OTHERS = sorted(
+    ((dz, dy) for dz in FAR for dy in FAR if (dz or dy) and (dz, dy) not in CORNER),
     key=lambda p: -(min(p[0], SIDE - p[0]) + min(p[1], SIDE - p[1])),
 )
 
@@ -59,8 +60,8 @@
     hidden_v, gain_v, wt_v, dt_v, xk_v, bck_v, ogain_v, ow_v, saved_v, xh_v, bch_v,
     hg_v, prod_v, fb_v,
     sa, sb, ra, rb, hs, hr,
-    pb, pr, ob, ro, qs, qr, qp, rq, ms,
-    accepted, load, sa_s, sb_s, hs_s, ra_s, rb_s, hr_s, pb_s, pr_s, qs_s, qr_s, ob_s, ro_s, qp_s, rq_s, ready,
+    wk, ws, sx, sr, ob, ro, qs, qr, qp, rq, ms,
+    accepted, load, sa_s, sb_s, hs_s, ra_s, rb_s, hr_s, ws_s, wr_s, sx_s, sr_s, qs_s, qr_s, ob_s, ro_s, qp_s, rq_s, near, ready,
 ):
     kv = lax.axis_index("kv")
     tp = lax.axis_index("tp")
@@ -71,6 +72,9 @@
     member = lax.rem(kv, 4)
     base = kv - member
 
+    def at(dz, dy):
+        return (lax.rem(z + dz, SIDE) * SIDE + lax.rem(y + dy, SIDE)) * 2 + core
+
     loads = []
 
     def fetch(src, dst):
@@ -93,13 +97,13 @@
     def greet(k, t):
         pl.semaphore_signal(barrier, inc=1, device_id=(k, t), device_id_type=MESH)
 
-    for d in range(1, SIDE):
-        greet((lax.rem(z + d, SIDE) * SIDE + y) * 2 + core, tp)
-        greet((z * SIDE + lax.rem(y + d, SIDE)) * 2 + core, tp)
-    for dm in range(4):
-        for dt in range(4):
+    for dt in (2, 1, 3, 0):
+        for dm in (2, 3, 1, 0):
             if dm or dt:
                 greet(base + lax.rem(member + dm, 4), lax.rem(tp + dt, 4))
+    for d in (3, 5, 2, 6, 1, 7):
+        greet(at(d, 0), tp)
+        greet(at(0, d), tp)
 
     l_hist = [fetch(accepted_h, accepted), fetch(xh, xh_v), fetch(bch, bch_v), fetch(xk, xk_v), fetch(bck, bck_v)]
     l_saved = fetch(saved, saved_v)
@@ -134,10 +138,18 @@
         tail = jnp.where(lane32 == 65, high, tail)
         tail = jnp.where(lane32 == 66, squares[i] - high, tail)
         prod_v[1, pl.ds(32 * i, 32), :] = tail
+    lane = iota((8, 128), 1)
+    low = lane < 64
     for i in range(4):
-        for part, out in ((0, sa), (1, sb)):
-            rows = [prod_v[part, pl.ds(32 * i + t, 8, stride=4), :] for t in range(4)]
-            out[i] = jnp.concatenate(rows, axis=0).astype(BF16)
+        rows = [prod_v[0, pl.ds(32 * i + t, 8, stride=4), :] for t in range(4)]
+        tails = [prod_v[1, pl.ds(32 * i + t, 8, stride=4), :] for t in range(4)]
+        misc = tails[0]
+        for t in range(1, 4):
+            misc = jnp.where(lane < 64 + 4 * t, misc, pltpu.roll(tails[t], 4 * t, 1))
+        sa[i] = jnp.concatenate([*rows, misc], axis=0).astype(BF16)
+        sb[i] = jnp.concatenate(
+            [jnp.where(low, tails[t], pltpu.roll(tails[t + 1], 64, 1)) for t in (0, 2)], axis=0
+        ).astype(BF16)
 
     for copy in l_hist:
         copy.wait()
@@ -164,15 +176,13 @@
     hr[member] = packed
     rb[4 * member] = sb[tp]
 
-    pl.semaphore_wait(barrier, 29)
-    for d in range(1, SIDE):
-        pl.semaphore_signal(
-            ready,
-            inc=1,
-            device_id=((lax.rem(z + d, SIDE) * SIDE + y) * 2 + core, tp),
-            device_id_type=MESH,
-        )
-
+    pl.semaphore_wait(barrier, 27)
+
+    def tell(sem, k):
+        pl.semaphore_signal(sem, inc=1, device_id=(k, tp), device_id_type=MESH)
+
+    tell(near, at(7, 0))
+    tell(near, at(0, 7))
     def send(src, dst, send_sem, recv_sem, k, t):
         copy = pltpu.make_async_remote_copy(
             src_ref=src,
@@ -203,6 +213,22 @@
         fb_v[pl.ds(64 * s, 64), :] = first.astype(BF16)
     l_ogain.wait()
     l_ow.wait()
+    quarter = lax.div(iota((64, 128), 1), 32)
+    flip = core == 1
+    for i in range(16):
+        left = ow_v[:, 256 * i : 256 * i + 128].astype(F32)
+        right = ow_v[:, 256 * i + 128 : 256 * i + 256].astype(F32)
+        left_64, right_32 = pltpu.roll(left, 64, 1), pltpu.roll(right, 32, 1)
+        left_96, right_64 = pltpu.roll(left, 96, 1), pltpu.roll(right, 64, 1)
+        first = jnp.where(quarter < 2, jnp.where(quarter == 0, left, left_96), jnp.where(quarter == 2, right_64, right_32))
+        second = jnp.where(quarter < 2, jnp.where(quarter == 0, left_96, left_64), jnp.where(quarter == 2, right_32, right))
+        wk[0:64, 128 * i : 128 * i + 128] = jnp.where(flip, second, first).astype(BF16)
+        ws[:, 128 * i : 128 * i + 128] = jnp.where(flip, first, second).astype(BF16)
+    partner = kv + 1 - 2 * core
+    send(ws, wk.at[pl.ds(64, 64)], ws_s, wr_s, partner, tp)
+    pl.semaphore_wait(near, 2)
+    for d in FAR[:-1]:
+        tell(ready, at(d, 0))
 
     wait_for(ra.at[pl.ds(1, 3)], ra_s)
     wait_for(rb.at[pl.ds(0, 15)], rb_s)
@@ -214,15 +240,22 @@
             out = out + block.astype(F32)
         return out
 
-    own = total([rb[4 * member + i] for i in range(4)])
-    square_sum = own[:, 65:66] + own[:, 66:67]
-    scale = jnp.broadcast_to(lax.rsqrt(square_sum / D + EPSILON), (32, 128))
-    xz = (total([sa[tp]] + [ra[i] for i in range(1, 4)]) * scale).astype(BF16).astype(F32)
-    dt_fresh = (own * scale).astype(BF16).astype(F32)[:, 64:65]
-    fresh = [
-        (total([rb[4 * m + i] for i in range(4)]) * scale).astype(BF16).astype(F32)[:, 0:64]
-        for m in range(4)
-    ]
+    def pieces(value):
+        return [value[8 * t : 8 * t + 8] for t in range(4)]
+
+    def spread(value, at):
+        return jnp.broadcast_to(value[:, at : at + 1], (8, 128))
+
+    def rounded(value):
+        return value.astype(BF16).astype(F32)
+
+    wide = total([sa[tp]] + [ra[i] for i in range(1, 4)])
+    misc = wide[32:40]
+    scales = lax.rsqrt((misc + pltpu.roll(misc, 127, 1)) / D + EPSILON)
+    dt_fresh = rounded(misc * pltpu.roll(scales, 127, 1))
+    scale = [spread(scales, 65 + 4 * t) for t in range(4)]
+    xz = [rounded(wide[8 * t : 8 * t + 8] * scale[t]) for t in range(4)]
+    fresh = [total([rb[4 * m + i] for i in range(4)]) for m in range(4)]
     stored = [hr[m].astype(F32)[:, 0:64] for m in range(4)]
 
     def conv(rows, taps):
@@ -234,21 +267,23 @@
             out.append(silu(value))
         return out
 
-    def pieces(value):
-        return [value[8 * t : 8 * t + 8] for t in range(4)]
-
-    x_rows = x_kept + pieces(xz[:, 0:64])
+    x_rows = x_kept + [value[:, 0:64] for value in xz]
     x_conv = conv(x_rows, xk_v[...].astype(F32))
     terms = []
-    for low, high in ((0, 1), (2, 3)):
-        new = pieces(jnp.concatenate([fresh[low], fresh[high]], axis=1))
-        old = jnp.concatenate([stored[low], stored[high]], axis=1)
-        taps = old[24:28]
-        terms.append(conv(pieces(old)[:3] + new, taps))
+    for left, right in ((0, 1), (2, 3)):
+        new = []
+        for t in (0, 2):
+            near, far = (fresh[m][4 * t : 4 * t + 8] for m in (left, right))
+            new.append(jnp.where(low, near, pltpu.roll(far, 64, 1)))
+            new.append(jnp.where(low, pltpu.roll(near, 64, 1), far))
+        new = [rounded(new[t] * scale[t]) for t in range(4)]
+        old = jnp.concatenate([stored[left], stored[right]], axis=1)
+        terms.append(conv(pieces(old)[:3] + new, old[24:28]))
     b_terms, c_terms = terms
 
     rate = jnp.exp(jnp.full((8, 128), decay_log[0], F32))
-    steps = pieces(softplus(jnp.broadcast_to(dt_fresh, (32, 128)) + dt_bias[0]))
+    all_steps = softplus(dt_fresh + dt_bias[0])
+    steps = [spread(all_steps, 64 + 4 * t) for t in range(4)]
     cumulated = []
     for t in range(4):
         value = -rate * steps[t]
@@ -267,7 +302,7 @@
     first_part = pieces(picked[:, 0:64] + picked[:, 64:128])
 
     gated = []
-    z_rows = pieces(xz[:, 64:128])
+    z_rows = [value[:, 64:128] for value in xz]
     for t in range(4):
         value = jnp.exp(cumulated[t])[:, 0:64] * first_part[t] + skip[0] * x_conv[t]
         for r in range(t + 1):
@@ -276,43 +311,44 @@
             value = value + weight[:, 0:64] * inner * x_conv[r]
         gated.append(value * silu(z_rows[t]))
     gated = jnp.concatenate(gated, axis=0)
+    scaled = (gated * ogain_v[...].astype(F32)).astype(BF16)
+    sx[...] = jnp.concatenate([scaled, jnp.zeros((32, 64), BF16)], axis=1)
+    send(sx, sr, sx_s, sr_s, partner, tp)
     square_sum = jnp.sum(gated * gated, axis=1, keepdims=True)
     diagonal = iota((32, 128), 0) == lane32
-    row = jnp.sum(jnp.where(diagonal, square_sum, 0.0), axis=0, keepdims=True)
-    qs[...] = row
-    partner = kv + 1 - 2 * core
+    qs[...] = jnp.sum(jnp.where(diagonal, square_sum, 0.0), axis=0, keepdims=True)
     send(qs, qr, qs_s, qr_s, partner, tp)
-    scaled = (gated * ogain_v[...].astype(F32)).astype(BF16)
-
-    for k in range(4):
-        for n in range(2 * k, 2 * k + 2):
-            partial = jnp.dot(
-                scaled, ow_v[:, 512 * n : 512 * n + 512], preferred_element_type=F32
-            )
-            for i in range(4):
-                tile = partial[:, 128 * i : 128 * i + 128]
-                blocks = transpose_blocks(pieces(tile))
-                for b in range(4):
-                    pb[b % 2, 2 * (4 * n + i) + b // 2] = blocks[b].astype(BF16)
-        part = pl.ds(16 * k, 16)
-        send(pb.at[1 - core, part], pr.at[part], pb_s.at[k], pr_s.at[k], partner, tp)
+    pl.semaphore_wait(ready, SIDE - 1)
 
     wait_for(qr, qr_s)
     qp[...] = qs[...] + qr[...]
-    pl.semaphore_wait(ready, SIDE - 1)
-
-    def at(dz, dy):
-        return lax.rem(z + dz, SIDE) * SIDE + lax.rem(y + dy, SIDE)
-
-    for dz, dy in STEPS:
-        send(qp, rq.at[dz * SIDE + dy], qp_s, rq_s, at(dz, dy) * 2 + core, tp)
-    for k in range(4):
-        part = pl.ds(16 * k, 16)
-        wait_for(pr.at[part], pr_s.at[k])
-        ob[part] = (pb[core, part].astype(F32) + pr[part].astype(F32)).astype(BF16)
-    for dz, dy in STEPS:
+    wait_for(wk.at[pl.ds(64, 64)], wr_s)
+    wait_for(sr, sr_s)
+
+    rows = jnp.concatenate([scaled, sr[:, 0:64]], axis=1)
+
+    def multiply(i):
+        start = pl.multiple_of(lax.rem(z + FAR[i], SIDE) * 256, 256)
+        partial = jnp.dot(rows, wk[:, pl.ds(start, 256)], preferred_element_type=F32)
+        for j in range(2):
+            blocks = transpose_blocks(pieces(partial[:, 128 * j : 128 * j + 128]))
+            for b in range(4):
+                ob[i, 4 * j + b] = blocks[b].astype(BF16)
+
+    def spread_out(dz, dy):
         to = at(dz, dy)
-        send(ob.at[to], ro.at[dz * SIDE + dy], ob_s, ro_s, to * 2 + core, tp)
+        slot = dz * SIDE + dy
+        send(ob.at[FAR.index(dz), lax.rem(y + dy, SIDE)], ro.at[slot], ob_s, ro_s, to, tp)
+        send(qp, rq.at[slot], qp_s, rq_s, to, tp)
+
+    for i in range(3):
+        multiply(i)
+    for dz, dy in CORNER:
+        spread_out(dz, dy)
+    for i in range(3, SIDE):
+        multiply(i)
+    for dz, dy in OTHERS:
+        spread_out(dz, dy)
 
     x_in = jnp.concatenate([x_conv[t] * steps[t][:, 0:64] for t in range(4)], axis=0)
     x_cols = jnp.transpose(jnp.concatenate([x_in, jnp.zeros((32, 64), F32)], axis=1))
@@ -325,16 +361,20 @@
             states[s, t + 1] = state
     for j in range(7):
         xwin[j] = x_rows[j].astype(BF16)
-    bc_rows = bc_kept + pieces((own * scale).astype(BF16).astype(F32)[:, 0:64])
+    own = total([rb[4 * member + i] for i in range(4)])
+    bc_rows = list(bc_kept)
+    for t in range(4):
+        half = own[8 * (t // 2) : 8 * (t // 2) + 8, 64 * (t % 2) : 64 * (t % 2) + 64]
+        bc_rows.append(rounded(half * scale[t][:, 0:64]))
     for j in range(7):
         bcwin[j] = bc_rows[j].astype(BF16)
 
-    wait_for(rq.at[pl.ds(1, CHIPS - 1)], rq_s)
-    squares_row = qp[...] + jnp.sum(rq[pl.ds(1, CHIPS - 1)], axis=0)
+    wait_for(rq.at[pl.ds(1, 63)], rq_s)
+    squares_row = qp[...] + jnp.sum(rq[pl.ds(1, 63)], axis=0)
     column = jnp.sum(jnp.where(diagonal, squares_row, 0.0), axis=1, keepdims=True)
     factor = lax.rsqrt(column / INNER + EPSILON)
-    wait_for(ro.at[pl.ds(1, CHIPS - 1)], ro_s)
-    summed = ob[chip].astype(F32) + jnp.sum(ro[pl.ds(1, CHIPS - 1)].astype(F32), axis=0)
+    wait_for(ro.at[pl.ds(1, 63)], ro_s)
+    summed = ob[7, y].astype(F32) + jnp.sum(ro[pl.ds(1, 63)].astype(F32), axis=0)
     for t in range(4):
         shifted = pltpu.roll(summed, (128 - 32 * t) % 128, 1) if t else summed
         ms[pl.ds(t, 8, stride=4), :] = shifted * factor[8 * t : 8 * t + 8]
@@ -343,11 +383,11 @@
     wait_for(sa.at[pl.ds(0, 3)], sa_s)
     wait_for(rb.at[pl.ds(0, 15)], sb_s)
     wait_for(hr.at[pl.ds(0, 3)], hs_s)
+    wait_for(ws, ws_s)
+    wait_for(sx, sx_s)
     wait_for(qs, qs_s)
-    for k in range(4):
-        wait_for(pr.at[pl.ds(16 * k, 16)], pb_s.at[k])
-    wait_for(rq.at[pl.ds(1, CHIPS - 1)], qp_s)
-    wait_for(ro.at[pl.ds(1, CHIPS - 1)], ob_s)
+    wait_for(ro.at[pl.ds(1, 63)], ob_s)
+    wait_for(rq.at[pl.ds(1, 63)], qp_s)
 
 
 def writer(mixed, states, xwin, bcwin, mixed_o, states_o, xwin_o, bcwin_o, sem):
@@ -371,17 +411,18 @@
 ):
     shapes = [((32, 32), BF16), ((8, 5, 64, 128), F32), ((7, 8, 64), BF16), ((7, 8, 64), BF16)]
     hbm = pl.BlockSpec(memory_space=pltpu.HBM)
+    smem = pl.BlockSpec(memory_space=pltpu.SMEM)
     vmem = pl.BlockSpec(memory_space=pltpu.VMEM)
-    smem = pl.BlockSpec(memory_space=pltpu.SMEM)
     dma = pltpu.SemaphoreType.DMA
     scratch = [
         ((128, 1024), BF16), ((8, 128), BF16), ((256, 1024), BF16), ((1, 1024), BF16),
         ((4, 64), BF16), ((4, 64), BF16), ((1, 64), BF16), ((64, 4096), BF16),
         ((8, 5, 64, 128), F32), ((7, 8, 64), BF16), ((7, 8, 64), BF16),
         ((128, 1024), BF16), ((2, 128, 128), F32), ((512, 128), BF16),
-        ((4, 32, 128), BF16), ((4, 32, 128), BF16), ((4, 32, 128), BF16), ((16, 32, 128), BF16),
+        ((4, 40, 128), BF16), ((4, 16, 128), BF16), ((4, 40, 128), BF16), ((16, 16, 128), BF16),
         ((32, 128), BF16), ((4, 32, 128), BF16),
-        ((2, 64, 8, 128), BF16), ((64, 8, 128), BF16), ((64, 8, 128), BF16), ((64, 8, 128), BF16),
+        ((128, 2048), BF16), ((64, 2048), BF16), ((32, 128), BF16), ((32, 128), BF16),
+        ((8, 8, 8, 128), BF16), ((64, 8, 128), BF16),
         ((1, 128), F32), ((1, 128), F32), ((1, 128), F32), ((64, 1, 128), F32), ((32, 128), F32),
     ]
     args = [
@@ -399,10 +440,8 @@
         out_specs=[vmem] * 4,
         scratch_shapes=[pltpu.VMEM(shape, dtype) for shape, dtype in scratch]
         + [pltpu.SMEM((8,), jnp.int32), dma((20,))]
-        + [dma(())] * 6
-        + [dma((4,)), dma((4,))]
-        + [dma(())] * 6
-        + [pltpu.SemaphoreType.REGULAR],
+        + [dma(())] * 16
+        + [pltpu.SemaphoreType.REGULAR] * 2,
         compiler_params=pltpu.CompilerParams(
             collective_id=0, has_side_effects=True, vmem_limit_bytes=24 << 20
         ),

time: 33.4 us -> 33.1 us (level)
  no operation moved by 1% of the time
where the time goes in v2:
time: 33.1 us; the launch traced here: 32.9 us
  Pallas kernels  30.3 us (92%)
  between operations  2.58 us (8%)
    pallas_call x1, Pallas kernels, local(): pl.pallas_call(mixer, name='mixer', out_shape=[pltpu.VMEM(shape, dtype) f...  29.2 us
    pallas_call x1, Pallas kernels, local(): pl.pallas_call(writer, name='writer', out_shape=[jax.ShapeDtypeStruct(sha...  1.12 us

profile of v2, /device:TPU:1, one launch (start us, length us, event | category | flops | bytes accessed | tf_op | source)
XLA Modules:
  0.0 32.9 jit_solution(10983627372010756045)
XLA Ops:
  2.6 29.2 %mixer.1 = (bf16[32,32]{1,0:T(8,128)(2,1)S(1)}, f32[8,5,64,128]{3,2,1,0:T(8,128)S(1)}, bf16[7,8,64]{2,1,0:T(8,128)(2,1)S(1)}, bf16[7,8,64]{2,1,0:T(8,128)(2,1)S(1)}) custom-call(bf16[128,1024]{1,0:T(8,128)(2,1)} %hidden.1, bf16[8,128]{1,0:T(8,128)(2,1)} %bitcast.21, bf16[64,1024]{1,0:T(8,128)(2,1)} %bitcast.15, bf16[64,1024]{1,0:T(8,128)(2,1)} %bitcast.16, ...), custom_call_target="tpu_custom_call" | custom-call | tf_op jit(solution)/shard_map/mixer/pallas_call | solution.py:435
  31.8 1.1 %writer.1 = (bf16[32,32]{1,0:T(8,128)(2,1)}, f32[8,5,64,128]{3,2,1,0:T(8,128)}, bf16[7,8,64]{2,1,0:T(8,128)(2,1)}, bf16[7,8,64]{2,1,0:T(8,128)(2,1)}) custom-call(bf16[32,32]{1,0:T(8,128)(2,1)S(1)} %get-tuple-element.12.mixed, f32[8,5,64,128]{3,2,1,0:T(8,128)S(1)} %get-tuple-element.13.states, bf16[7,8,64]{2,1,0:T(8,128)(2,1)S(1)} %get-tuple-element.14.xwin, ...), custom_call_target="tpu_custom_call" | custom-call | tf_op jit(solution)/shard_map/writer/pallas_call | solution.py:449

commit v3 on v2

--- a/solution.py
+++ b/solution.py
@@ -317,11 +317,10 @@
     square_sum = jnp.sum(gated * gated, axis=1, keepdims=True)
     diagonal = iota((32, 128), 0) == lane32
     qs[...] = jnp.sum(jnp.where(diagonal, square_sum, 0.0), axis=0, keepdims=True)
-    send(qs, qr, qs_s, qr_s, partner, tp)
     pl.semaphore_wait(ready, SIDE - 1)
-
-    wait_for(qr, qr_s)
-    qp[...] = qs[...] + qr[...]
+    for dz, dy in CORNER + OTHERS:
+        send(qs, rq.at[dz * SIDE + dy], qs_s, rq_s, at(dz, dy), tp)
+
     wait_for(wk.at[pl.ds(64, 64)], wr_s)
     wait_for(sr, sr_s)
 
@@ -336,10 +335,8 @@
                 ob[i, 4 * j + b] = blocks[b].astype(BF16)
 
     def spread_out(dz, dy):
-        to = at(dz, dy)
-        slot = dz * SIDE + dy
-        send(ob.at[FAR.index(dz), lax.rem(y + dy, SIDE)], ro.at[slot], ob_s, ro_s, to, tp)
-        send(qp, rq.at[slot], qp_s, rq_s, to, tp)
+        block = ob.at[FAR.index(dz), lax.rem(y + dy, SIDE)]
+        send(block, ro.at[dz * SIDE + dy], ob_s, ro_s, at(dz, dy), tp)
 
     for i in range(3):
         multiply(i)
@@ -370,11 +367,14 @@
         bcwin[j] = bc_rows[j].astype(BF16)
 
     wait_for(rq.at[pl.ds(1, 63)], rq_s)
-    squares_row = qp[...] + jnp.sum(rq[pl.ds(1, 63)], axis=0)
+    qp[...] = qs[...] + jnp.sum(rq[pl.ds(1, 63)], axis=0)
+    send(qp, qr, qp_s, qr_s, partner, tp)
+    wait_for(ro.at[pl.ds(1, 63)], ro_s)
+    summed = ob[7, y].astype(F32) + jnp.sum(ro[pl.ds(1, 63)].astype(F32), axis=0)
+    wait_for(qr, qr_s)
+    squares_row = qp[...] + qr[...]
     column = jnp.sum(jnp.where(diagonal, squares_row, 0.0), axis=1, keepdims=True)
     factor = lax.rsqrt(column / INNER + EPSILON)
-    wait_for(ro.at[pl.ds(1, 63)], ro_s)
-    summed = ob[7, y].astype(F32) + jnp.sum(ro[pl.ds(1, 63)].astype(F32), axis=0)
     for t in range(4):
         shifted = pltpu.roll(summed, (128 - 32 * t) % 128, 1) if t else summed
         ms[pl.ds(t, 8, stride=4), :] = shifted * factor[8 * t : 8 * t + 8]
@@ -385,9 +385,9 @@
     wait_for(hr.at[pl.ds(0, 3)], hs_s)
     wait_for(ws, ws_s)
     wait_for(sx, sx_s)
-    wait_for(qs, qs_s)
+    wait_for(rq.at[pl.ds(1, 63)], qs_s)
     wait_for(ro.at[pl.ds(1, 63)], ob_s)
-    wait_for(rq.at[pl.ds(1, 63)], qp_s)
+    wait_for(qp, qp_s)
 
 
 def writer(mixed, states, xwin, bcwin, mixed_o, states_o, xwin_o, bcwin_o, sem):

time: 33.1 us -> 32.3 us (0.976)
  Pallas kernels: 30.3 us -> 29.6 us
    pallas_call x1, Pallas kernels: 29.2 us -> 28.5 us  [local(): pl.pallas_call(mixer, name='mixer', out_shape=[pltpu.VMEM(shape, dtype) f...]
where the time goes in v3:
time: 32.3 us; the launch traced here: 32.2 us
  Pallas kernels  29.6 us (92%)
  between operations  2.58 us (8%)
    pallas_call x1, Pallas kernels, local(): pl.pallas_call(mixer, name='mixer', out_shape=[pltpu.VMEM(shape, dtype) f...  28.5 us
    pallas_call x1, Pallas kernels, local(): pl.pallas_call(writer, name='writer', out_shape=[jax.ShapeDtypeStruct(sha...  1.12 us

profile of v3, /device:TPU:1, one launch (start us, length us, event | category | flops | bytes accessed | tf_op | source)
XLA Modules:
  0.0 32.2 jit_solution(2397302199609601250)
XLA Ops:
  2.6 28.5 %mixer.1 = (bf16[32,32]{1,0:T(8,128)(2,1)S(1)}, f32[8,5,64,128]{3,2,1,0:T(8,128)S(1)}, bf16[7,8,64]{2,1,0:T(8,128)(2,1)S(1)}, bf16[7,8,64]{2,1,0:T(8,128)(2,1)S(1)}) custom-call(bf16[128,1024]{1,0:T(8,128)(2,1)} %hidden.1, bf16[8,128]{1,0:T(8,128)(2,1)} %bitcast.21, bf16[64,1024]{1,0:T(8,128)(2,1)} %bitcast.15, bf16[64,1024]{1,0:T(8,128)(2,1)} %bitcast.16, ...), custom_call_target="tpu_custom_call" | custom-call | tf_op jit(solution)/shard_map/mixer/pallas_call | solution.py:435
  31.0 1.1 %writer.1 = (bf16[32,32]{1,0:T(8,128)(2,1)}, f32[8,5,64,128]{3,2,1,0:T(8,128)}, bf16[7,8,64]{2,1,0:T(8,128)(2,1)}, bf16[7,8,64]{2,1,0:T(8,128)(2,1)}) custom-call(bf16[32,32]{1,0:T(8,128)(2,1)S(1)} %get-tuple-element.12.mixed, f32[8,5,64,128]{3,2,1,0:T(8,128)S(1)} %get-tuple-element.13.states, bf16[7,8,64]{2,1,0:T(8,128)(2,1)S(1)} %get-tuple-element.14.xwin, ...), custom_call_target="tpu_custom_call" | custom-call | tf_op jit(solution)/shard_map/writer/pallas_call | solution.py:449

commit v4 on v2

--- a/solution.py
+++ b/solution.py
@@ -13,11 +13,9 @@
 BF16 = jnp.bfloat16
 SIDE = 8
 FAR = (4, 3, 5, 2, 6, 1, 7, 0)
-CORNER = [(dz, dy) for dz in FAR[:3] for dy in FAR[:3]]
-OTHERS = sorted(
-    ((dz, dy) for dz in FAR for dy in FAR if (dz or dy) and (dz, dy) not in CORNER),
-    key=lambda p: -(min(p[0], SIDE - p[0]) + min(p[1], SIDE - p[1])),
-)
+ALONG = (1, 4, 2, 3, 5, 6, 7, 0)
+EARLY = [(dz, dy) for pair in (ALONG[:2], ALONG[2:4]) for dy in FAR for dz in pair]
+LATE = [(dz, dy) for dz in ALONG[4:] for dy in FAR if dz or dy]
 
 
 def iota(shape, dim):
@@ -328,7 +326,7 @@
     rows = jnp.concatenate([scaled, sr[:, 0:64]], axis=1)
 
     def multiply(i):
-        start = pl.multiple_of(lax.rem(z + FAR[i], SIDE) * 256, 256)
+        start = pl.multiple_of(lax.rem(z + ALONG[i], SIDE) * 256, 256)
         partial = jnp.dot(rows, wk[:, pl.ds(start, 256)], preferred_element_type=F32)
         for j in range(2):
             blocks = transpose_blocks(pieces(partial[:, 128 * j : 128 * j + 128]))
@@ -338,16 +336,16 @@
     def spread_out(dz, dy):
         to = at(dz, dy)
         slot = dz * SIDE + dy
-        send(ob.at[FAR.index(dz), lax.rem(y + dy, SIDE)], ro.at[slot], ob_s, ro_s, to, tp)
+        send(ob.at[ALONG.index(dz), lax.rem(y + dy, SIDE)], ro.at[slot], ob_s, ro_s, to, tp)
         send(qp, rq.at[slot], qp_s, rq_s, to, tp)
 
-    for i in range(3):
+    for i in range(4):
         multiply(i)
-    for dz, dy in CORNER:
+    for dz, dy in EARLY:
         spread_out(dz, dy)
-    for i in range(3, SIDE):
+    for i in range(4, SIDE):
         multiply(i)
-    for dz, dy in OTHERS:
+    for dz, dy in LATE:
         spread_out(dz, dy)
 
     x_in = jnp.concatenate([x_conv[t] * steps[t][:, 0:64] for t in range(4)], axis=0)

time: 33.1 us -> 32.6 us (0.985)
  Pallas kernels: 30.3 us -> 29.9 us
    pallas_call x1, Pallas kernels: 29.2 us -> 28.8 us  [local(): pl.pallas_call(mixer, name='mixer', out_shape=[pltpu.VMEM(shape, dtype) f...]
where the time goes in v4:
time: 32.6 us; the launch traced here: 32.5 us
  Pallas kernels  29.9 us (92%)
  between operations  2.58 us (8%)
    pallas_call x1, Pallas kernels, local(): pl.pallas_call(mixer, name='mixer', out_shape=[pltpu.VMEM(shape, dtype) f...  28.8 us
    pallas_call x1, Pallas kernels, local(): pl.pallas_call(writer, name='writer', out_shape=[jax.ShapeDtypeStruct(sha...  1.12 us

profile of v4, /device:TPU:1, one launch (start us, length us, event | category | flops | bytes accessed | tf_op | source)
XLA Modules:
  0.0 32.5 jit_solution(15859031679224483493)
XLA Ops:
  2.6 28.8 %mixer.1 = (bf16[32,32]{1,0:T(8,128)(2,1)S(1)}, f32[8,5,64,128]{3,2,1,0:T(8,128)S(1)}, bf16[7,8,64]{2,1,0:T(8,128)(2,1)S(1)}, bf16[7,8,64]{2,1,0:T(8,128)(2,1)S(1)}) custom-call(bf16[128,1024]{1,0:T(8,128)(2,1)} %hidden.1, bf16[8,128]{1,0:T(8,128)(2,1)} %bitcast.21, bf16[64,1024]{1,0:T(8,128)(2,1)} %bitcast.15, bf16[64,1024]{1,0:T(8,128)(2,1)} %bitcast.16, ...), custom_call_target="tpu_custom_call" | custom-call | tf_op jit(solution)/shard_map/mixer/pallas_call | solution.py:433
  31.3 1.1 %writer.1 = (bf16[32,32]{1,0:T(8,128)(2,1)}, f32[8,5,64,128]{3,2,1,0:T(8,128)}, bf16[7,8,64]{2,1,0:T(8,128)(2,1)}, bf16[7,8,64]{2,1,0:T(8,128)(2,1)}) custom-call(bf16[32,32]{1,0:T(8,128)(2,1)S(1)} %get-tuple-element.12.mixed, f32[8,5,64,128]{3,2,1,0:T(8,128)S(1)} %get-tuple-element.13.states, bf16[7,8,64]{2,1,0:T(8,128)(2,1)S(1)} %get-tuple-element.14.xwin, ...), custom_call_target="tpu_custom_call" | custom-call | tf_op jit(solution)/shard_map/writer/pallas_call | solution.py:447

commit v5 on v3

--- a/solution.py
+++ b/solution.py
@@ -13,11 +13,9 @@
 BF16 = jnp.bfloat16
 SIDE = 8
 FAR = (4, 3, 5, 2, 6, 1, 7, 0)
-CORNER = [(dz, dy) for dz in FAR[:3] for dy in FAR[:3]]
-OTHERS = sorted(
-    ((dz, dy) for dz in FAR for dy in FAR if (dz or dy) and (dz, dy) not in CORNER),
-    key=lambda p: -(min(p[0], SIDE - p[0]) + min(p[1], SIDE - p[1])),
-)
+ALONG = (1, 4, 2, 3, 5, 6, 7, 0)
+EARLY = [(dz, dy) for dy in FAR for dz in ALONG[:2]]
+LATE = [(dz, dy) for dy in FAR for dz in ALONG[2:] if dz or dy]
 
 
 def iota(shape, dim):
@@ -318,7 +316,7 @@
     diagonal = iota((32, 128), 0) == lane32
     qs[...] = jnp.sum(jnp.where(diagonal, square_sum, 0.0), axis=0, keepdims=True)
     pl.semaphore_wait(ready, SIDE - 1)
-    for dz, dy in CORNER + OTHERS:
+    for dz, dy in EARLY + LATE:
         send(qs, rq.at[dz * SIDE + dy], qs_s, rq_s, at(dz, dy), tp)
 
     wait_for(wk.at[pl.ds(64, 64)], wr_s)
@@ -327,7 +325,7 @@
     rows = jnp.concatenate([scaled, sr[:, 0:64]], axis=1)
 
     def multiply(i):
-        start = pl.multiple_of(lax.rem(z + FAR[i], SIDE) * 256, 256)
+        start = pl.multiple_of(lax.rem(z + ALONG[i], SIDE) * 256, 256)
         partial = jnp.dot(rows, wk[:, pl.ds(start, 256)], preferred_element_type=F32)
         for j in range(2):
             blocks = transpose_blocks(pieces(partial[:, 128 * j : 128 * j + 128]))
@@ -335,16 +333,16 @@
                 ob[i, 4 * j + b] = blocks[b].astype(BF16)
 
     def spread_out(dz, dy):
-        block = ob.at[FAR.index(dz), lax.rem(y + dy, SIDE)]
+        block = ob.at[ALONG.index(dz), lax.rem(y + dy, SIDE)]
         send(block, ro.at[dz * SIDE + dy], ob_s, ro_s, at(dz, dy), tp)
 
-    for i in range(3):
+    for i in range(2):
         multiply(i)
-    for dz, dy in CORNER:
+    for dz, dy in EARLY:
         spread_out(dz, dy)
-    for i in range(3, SIDE):
+    for i in range(2, SIDE):
         multiply(i)
-    for dz, dy in OTHERS:
+    for dz, dy in LATE:
         spread_out(dz, dy)
 
     x_in = jnp.concatenate([x_conv[t] * steps[t][:, 0:64] for t in range(4)], axis=0)

time: 32.3 us -> 31.9 us (0.988)
  Pallas kernels: 29.6 us -> 29.1 us
    pallas_call x1, Pallas kernels: 28.5 us -> 28 us  [local(): pl.pallas_call(mixer, name='mixer', out_shape=[pltpu.VMEM(shape, dtype) f...]
where the time goes in v5:
time: 31.9 us; the launch traced here: 31.7 us
  Pallas kernels  29.1 us (91%)
  between operations  2.58 us (8%)
    pallas_call x1, Pallas kernels, local(): pl.pallas_call(mixer, name='mixer', out_shape=[pltpu.VMEM(shape, dtype) f...  28 us
    pallas_call x1, Pallas kernels, local(): pl.pallas_call(writer, name='writer', out_shape=[jax.ShapeDtypeStruct(sha...  1.12 us

profile of v5, /device:TPU:1, one launch (start us, length us, event | category | flops | bytes accessed | tf_op | source)
XLA Modules:
  0.0 31.7 jit_solution(15522202276293037239)
XLA Ops:
  2.6 28.0 %mixer.1 = (bf16[32,32]{1,0:T(8,128)(2,1)S(1)}, f32[8,5,64,128]{3,2,1,0:T(8,128)S(1)}, bf16[7,8,64]{2,1,0:T(8,128)(2,1)S(1)}, bf16[7,8,64]{2,1,0:T(8,128)(2,1)S(1)}) custom-call(bf16[128,1024]{1,0:T(8,128)(2,1)} %hidden.1, bf16[8,128]{1,0:T(8,128)(2,1)} %bitcast.21, bf16[64,1024]{1,0:T(8,128)(2,1)} %bitcast.15, bf16[64,1024]{1,0:T(8,128)(2,1)} %bitcast.16, ...), custom_call_target="tpu_custom_call" | custom-call | tf_op jit(solution)/shard_map/mixer/pallas_call | solution.py:433
  30.6 1.1 %writer.1 = (bf16[32,32]{1,0:T(8,128)(2,1)}, f32[8,5,64,128]{3,2,1,0:T(8,128)}, bf16[7,8,64]{2,1,0:T(8,128)(2,1)}, bf16[7,8,64]{2,1,0:T(8,128)(2,1)}) custom-call(bf16[32,32]{1,0:T(8,128)(2,1)S(1)} %get-tuple-element.12.mixed, f32[8,5,64,128]{3,2,1,0:T(8,128)S(1)} %get-tuple-element.13.states, bf16[7,8,64]{2,1,0:T(8,128)(2,1)S(1)} %get-tuple-element.14.xwin, ...), custom_call_target="tpu_custom_call" | custom-call | tf_op jit(solution)/shard_map/writer/pallas_call | solution.py:447
